TPU v7x, 32 devices: a whole 2x2x4 slice. The times are simulated.
32 devices in a mesh: kv: 8 (over z, y), tp: 4 (over x, core).
Axes of the slice: x: 2, y: 2, z: 4, core: 2. Of those that a mesh axis runs over, the one named last changes fastest.
Arguments:
- residual: bfloat16 [256, 2048], P('kv', 'tp'), may hold values from -12 to 12
- first_gain: bfloat16 [2048], P('tp'), may hold values from 0.099609375 to 1.8984375
- first_gate: bfloat16 [2048, 5632], P('tp', 'kv'), may hold values from -0.125 to 0.125
- first_lift: bfloat16 [2048, 5632], P('tp', 'kv'), may hold values from -0.125 to 0.125
- first_down: bfloat16 [5632, 2048], P('kv', 'tp'), may hold values from -0.078125 to 0.078125
- mixer_gain: bfloat16 [2048], replicated, may hold values from 0.099609375 to 1.8984375
- proj_gate: bfloat16 [2048, 2048], P(None, 'tp'), may hold values from -0.125 to 0.125
- proj_input: bfloat16 [2048, 2048], P(None, 'tp'), may hold values from -0.125 to 0.125
- proj_write: bfloat16 [2048, 1024], P(None, 'tp'), may hold values from -0.125 to 0.125
- proj_read: bfloat16 [2048, 1024], P(None, 'tp'), may hold values from -0.125 to 0.125
- proj_step: bfloat16 [2048, 32], P(None, 'tp'), may hold values from -0.125 to 0.125
- step_bias: float32 [32], P('tp'), may hold values from -5 to -2
- rate_log: float32 [32], P('tp'), may hold values from -0.7 to 2.1
- skip_gain: float32 [32], P('tp'), may hold values from 0.5 to 2
- taps_input: bfloat16 [4, 2048], P(None, 'tp'), may hold values from -3 to 3
- taps_write: bfloat16 [4, 1024], P(None, 'tp'), may hold values from -3 to 3
- taps_read: bfloat16 [4, 1024], P(None, 'tp'), may hold values from -3 to 3
- buffer_input: bfloat16 [256, 3, 2048], P('kv', None, 'tp'), may hold values from -6 to 6
- buffer_write: bfloat16 [256, 3, 1024], P('kv', None, 'tp'), may hold values from -6 to 6
- buffer_read: bfloat16 [256, 3, 1024], P('kv', None, 'tp'), may hold values from -6 to 6
- scan_state: float32 [256, 32, 64, 128], P('kv', 'tp'), may hold values from -1.5 to 1.5
- group_gain: bfloat16 [2048], P('tp'), may hold values from 0.099609375 to 1.8984375
- proj_output: bfloat16 [2048, 2048], P('tp'), may hold values from -0.125 to 0.125
- second_gain: bfloat16 [2048], P('tp'), may hold values from 0.099609375 to 1.8984375
- second_gate: bfloat16 [2048, 5632], P('tp', 'kv'), may hold values from -0.125 to 0.125
- second_lift: bfloat16 [2048, 5632], P('tp', 'kv'), may hold values from -0.125 to 0.125
- second_down: bfloat16 [5632, 2048], P('kv', 'tp'), may hold values from -0.078125 to 0.078125
Outputs:
- residual_out: bfloat16 [256, 2048], P('kv', 'tp')
- state_out: float32 [256, 32, 64, 128], P('kv', 'tp')
All inputs are finite; a program needn't handle non-finite values.
Results may differ from a plain program's by a relative error of at most 0.023.
Values may be sent and summed in bfloat16 or wider, within the bound.
A program may use at most 64 MiB of HBM per device.

v0:
```python
import jax
import jax.numpy as jnp
from jax import lax
from jax.sharding import PartitionSpec as P

D = 2048
HEAD_DIM = 64
STATE = 128
norm_eps = 1e-06


def inverse_rms(values):
    return lax.rsqrt(jnp.mean(values * values, axis=-1, keepdims=True) + norm_eps)


def half_step(residual, gain, gate_weight, lift_weight, down_weight):
    widened = residual.astype(jnp.float32)
    row_total = lax.psum(jnp.sum(widened * widened, axis=1), "tp")
    factor = lax.rsqrt(row_total / D + norm_eps)
    normed = (widened * factor[:, None] * gain.astype(jnp.float32)[None, :]).astype(jnp.bfloat16)
    hidden_cols = gate_weight.shape[1]
    row_piece = lax.all_gather(normed, "kv", axis=0, tiled=True)
    gate_part = jnp.dot(row_piece, gate_weight, preferred_element_type=jnp.float32).astype(
        jnp.bfloat16
    )
    lift_part = jnp.dot(row_piece, lift_weight, preferred_element_type=jnp.float32).astype(
        jnp.bfloat16
    )
    joined = lax.optimization_barrier(jnp.concatenate([gate_part, lift_part], axis=1))
    partial_value = joined.astype(jnp.float32)
    share = lax.psum_scatter(
        partial_value.astype(jnp.bfloat16), "tp", scatter_dimension=0, tiled=True
    ).astype(jnp.float32)
    active = (jax.nn.silu(share[:, :hidden_cols]) * share[:, hidden_cols:]).astype(jnp.bfloat16)
    hidden = lax.all_gather(active, "tp", axis=0, tiled=True)
    branch = lax.psum_scatter(
        jnp.dot(hidden, down_weight, preferred_element_type=jnp.float32).astype(jnp.bfloat16),
        "kv",
        scatter_dimension=0,
        tiled=True,
    ).astype(jnp.float32)
    return (widened + 0.5 * branch).astype(jnp.bfloat16)


def short_conv(tap_weights, buffer, newest):
    taps_f = tap_weights.astype(jnp.float32)
    summed = jnp.sum(buffer.astype(jnp.float32) * taps_f[None, :-1, :], axis=1)
    summed = summed + newest.astype(jnp.float32) * taps_f[-1][None, :]
    return jax.nn.silu(summed)


def state_mixer(
    residual,
    mixer_gain,
    proj_gate,
    proj_input,
    proj_write,
    proj_read,
    proj_step,
    step_bias,
    rate_log,
    skip_gain,
    taps_input,
    taps_write,
    taps_read,
    buffer_input,
    buffer_write,
    buffer_read,
    scan_state,
    group_gain,
    proj_output,
):
    seq_rows = residual.shape[0]
    full_rows = lax.all_gather(residual, "tp", axis=1, tiled=True)
    widened = full_rows.astype(jnp.float32)
    normed = (widened * inverse_rms(widened) * mixer_gain.astype(jnp.float32)[None, :]).astype(
        jnp.bfloat16
    )

    def state_project(weight):
        return jnp.dot(normed, weight, preferred_element_type=jnp.float32).astype(jnp.bfloat16)

    gate_z = state_project(proj_gate)
    input_new = state_project(proj_input)
    write_new = state_project(proj_write)
    read_new = state_project(proj_read)
    step_raw = state_project(proj_step)
    input_conv = short_conv(taps_input, buffer_input, input_new)
    write_conv = short_conv(taps_write, buffer_write, write_new)
    read_conv = short_conv(taps_read, buffer_read, read_new)
    head_count = proj_step.shape[1]
    group_count = proj_write.shape[1] // STATE
    per_group = head_count // group_count
    step = jax.nn.softplus(step_raw.astype(jnp.float32) + step_bias[None, :])
    retain = jnp.exp(-step * jnp.exp(rate_log)[None, :])
    input_heads = input_conv.reshape(seq_rows, group_count, per_group, HEAD_DIM)
    write_groups = write_conv.reshape(seq_rows, group_count, STATE)
    read_groups = read_conv.reshape(seq_rows, group_count, STATE)
    old_state = scan_state.reshape(seq_rows, group_count, per_group, HEAD_DIM, STATE)
    retain_g = retain.reshape(seq_rows, group_count, per_group)
    step_g = step.reshape(seq_rows, group_count, per_group)
    updated = (
        retain_g[..., None, None] * old_state
        + (step_g[..., None] * input_heads)[..., None] * write_groups[:, :, None, None, :]
    )
    head_out = jnp.einsum("bgrpn,bgn->bgrp", updated, read_groups, precision=lax.Precision.HIGHEST)
    head_out = head_out + skip_gain.reshape(group_count, per_group)[None, :, :, None] * input_heads
    head_short = lax.optimization_barrier(head_out.astype(jnp.bfloat16))
    gated = head_short.astype(jnp.float32).reshape(seq_rows, group_count, per_group * HEAD_DIM)
    gated = gated * jax.nn.silu(
        gate_z.astype(jnp.float32).reshape(seq_rows, group_count, per_group * HEAD_DIM)
    )
    gated = (
        gated
        * inverse_rms(gated)
        * group_gain.astype(jnp.float32).reshape(group_count, per_group * HEAD_DIM)[None]
    )
    gated = gated.reshape(seq_rows, head_count * HEAD_DIM).astype(jnp.bfloat16)
    partial_out = jnp.dot(gated, proj_output, preferred_element_type=jnp.float32).astype(
        jnp.bfloat16
    )
    partial_out = lax.optimization_barrier(partial_out).astype(jnp.float32)
    mixed = lax.psum_scatter(
        partial_out.astype(jnp.bfloat16), "tp", scatter_dimension=1, tiled=True
    ).astype(jnp.float32)
    mixed_rows = (residual.astype(jnp.float32) + mixed).astype(jnp.bfloat16)
    return (mixed_rows, updated.reshape(seq_rows, head_count, HEAD_DIM, STATE))


def per_device(
    residual,
    first_gain,
    first_gate,
    first_lift,
    first_down,
    mixer_gain,
    proj_gate,
    proj_input,
    proj_write,
    proj_read,
    proj_step,
    step_bias,
    rate_log,
    skip_gain,
    taps_input,
    taps_write,
    taps_read,
    buffer_input,
    buffer_write,
    buffer_read,
    scan_state,
    group_gain,
    proj_output,
    second_gain,
    second_gate,
    second_lift,
    second_down,
):
    first = half_step(residual, first_gain, first_gate, first_lift, first_down)
    mixed, state_out = state_mixer(
        first,
        mixer_gain,
        proj_gate,
        proj_input,
        proj_write,
        proj_read,
        proj_step,
        step_bias,
        rate_log,
        skip_gain,
        taps_input,
        taps_write,
        taps_read,
        buffer_input,
        buffer_write,
        buffer_read,
        scan_state,
        group_gain,
        proj_output,
    )
    residual_out = half_step(mixed, second_gain, second_gate, second_lift, second_down)
    return (residual_out, state_out)


def solution(mesh):
    placed = (
        P("kv", "tp"),
        P("tp"),
        P("tp", "kv"),
        P("tp", "kv"),
        P("kv", "tp"),
        P(),
        P(None, "tp"),
        P(None, "tp"),
        P(None, "tp"),
        P(None, "tp"),
        P(None, "tp"),
        P("tp"),
        P("tp"),
        P("tp"),
        P(None, "tp"),
        P(None, "tp"),
        P(None, "tp"),
        P("kv", None, "tp"),
        P("kv", None, "tp"),
        P("kv", None, "tp"),
        P("kv", "tp", None, None),
        P("tp"),
        P("tp", None),
        P("tp"),
        P("tp", "kv"),
        P("tp", "kv"),
        P("kv", "tp"),
    )
    return jax.shard_map(
        per_device,
        mesh=mesh,
        in_specs=placed,
        out_specs=(P("kv", "tp"), P("kv", "tp", None, None)),
        check_vma=False,
    )
```

profile of v0, /device:TPU:0, one launch (start us, length us, event | category | flops | bytes accessed | tf_op | source)
XLA Modules:
  0.0 352.4 jit_solution(14504042245031635717)
XLA Ops:
  7.3 0.0 reduce-scatter.16.cloned.1.call-start
  7.4 1.1 fusion.27
  8.4 8.4 %psum.14 = f32[32]{0:T(128)S(1)} all-reduce(f32[32]{0:T(128)S(1)} %fusion.27), channel_id=1, replica_groups=mesh['kv'=8,'tp'=4] {'tp'}, use_global_device_ids=true, to_apply=%region_1.0 | all-reduce | flops 32 | bytes 256 | tf_op jit(solution)/shard_map/psum | solution.py:18
  16.8 0.7 convert_element_type.148
  17.5 0.8 fusion.29
  18.3 31.2 %all_gather.15 = bf16[256,512]{1,0:T(8,128)(2,1)S(1)} all-gather(bf16[32,512]{1,0:T(8,128)(2,1)S(1)} %fusion.29), channel_id=1, replica_groups=mesh['kv'=8,'tp'=4] {'kv'}, dimensions={0}, use_global_device_ids=true | all-gather | bytes 294912 | tf_op jit(solution)/shard_map/all_gather | solution.py:22
  49.5 1.5 convolution_convert_fusion.3
  51.0 1.5 convolution_convert_fusion.4
  52.6 1.1 copy.47
  53.7 0.0 reduce-scatter.16.cloned.1.call-update
  53.8 0.0 reduce-scatter.10.cloned.1.call-start
  53.8 22.8 %reduce-scatter.16.cloned.1.call-done = bf16[64,1408]{1,0:T(8,128)(2,1)} async-done(((bf16[256,1408]{1,0:T(8,128)(2,1)}), bf16[64,1408]{1,0:T(8,128)(2,1)}) %reduce-scatter.16.cloned.1.call-update) | async-done | bytes 180240 | tf_op jit(solution)/shard_map/reduce_scatter | solution.py:31
  76.6 0.9 convert_element_type.152
  77.5 0.1 fusion.23
  77.6 6.1 %all_gather.16 = bf16[256,704]{1,0:T(8,128)(2,1)S(1)} all-gather(bf16[64,704]{1,0:T(8,128)(2,1)S(1)} %fusion.23), channel_id=1, replica_groups=mesh['kv'=8,'tp'=4] {'tp'}, dimensions={0}, use_global_device_ids=true | all-gather | bytes 450560 | tf_op jit(solution)/shard_map/all_gather | solution.py:35
  83.8 2.2 convolution_convert_fusion.6
  86.0 0.0 reduce-scatter.10.cloned.1.call-update
  86.0 0.0 reduce-scatter.12.cloned.1.call-start
  86.2 0.1 mul.301
  86.4 62.7 %reduce-scatter.10.cloned.1.call-done = bf16[32,512]{1,0:T(8,128)(2,1)} async-done(((bf16[256,512]{1,0:T(8,128)(2,1)}), bf16[32,512]{1,0:T(8,128)(2,1)}) %reduce-scatter.10.cloned.1.call-update) | async-done | bytes 32784 | tf_op jit(solution)/shard_map/reduce_scatter | solution.py:36
  149.1 0.8 fusion.30
  149.9 5.4 %all_gather.17 = bf16[32,2048]{1,0:T(8,128)(2,1)S(1)} all-gather(bf16[32,512]{1,0:T(8,128)(2,1)S(1)} %fusion.30), channel_id=1, replica_groups=mesh['kv'=8,'tp'=4] {'tp'}, dimensions={1}, use_global_device_ids=true | all-gather | bytes 163840 | tf_op jit(solution)/shard_map/all_gather | solution.py:74
  155.3 0.1 fusion.19
  155.4 1.6 divide_multiply_fusion.3
  157.0 1.6 divide_multiply_fusion.2
  158.6 2.1 fusion.7
  160.8 0.2 multiply_exponential_fusion
  161.0 0.1 copy.41
  161.1 0.1 copy.40
  161.2 2.1 divide_multiply_fusion.1
  163.4 0.1 reshape.73
  163.5 0.1 broadcast_multiply_fusion.1
  163.6 22.0 %fusion = f32[32,2,1,4,64]{4,2,3,1,0:T(1,128)S(1)} fusion(f32[32,2,128,1,1]{2,3,4,1,0:T(1,128)S(1)} %bitcast.38, f32[32,2,4,64,128]{4,3,2,1,0:T(8,128)} %bitcast.33, f32[32,2,128]{2,1,0:T(2,128)S(1)} %mul.292, f32[32,2,4,64]{3,2,1,0:T(4,128)S(1)} %broadcast_multiply_fusion.1, f32[32,2,4]{2,1,0:T(2,128)S(1)} %copy.40), kind=kOutput, calls=%fused_computation.1 | convolution fusion | flops 31457280 | bytes 8586240 | tf_op jit(solution)/shard_map/bgrpn,bgn->bgrp/dot_general | solution.py:106
  185.6 0.1 add_convert_fusion
  185.8 0.1 reshape.75
  185.9 0.1 reshape.76
  186.0 0.2 fusion.26
  186.2 0.1 mul.309
  186.4 1.1 convolution_convert_fusion
  187.5 0.0 reduce-scatter.12.cloned.1.call-update
  187.5 0.0 reduce-scatter.18.cloned.1.call-start
  187.6 18.7 %reduce-scatter.12.cloned.1.call-done = bf16[32,512]{1,0:T(8,128)(2,1)} async-done(((bf16[32,2048]{1,0:T(8,128)(2,1)}), bf16[32,512]{1,0:T(8,128)(2,1)}) %reduce-scatter.12.cloned.1.call-update) | async-done | bytes 32784 | tf_op jit(solution)/shard_map/reduce_scatter | solution.py:123
  206.3 0.9 fusion.31
  207.2 5.8 %psum.15 = f32[32]{0:T(128)S(1)} all-reduce(f32[32]{0:T(128)S(1)} %fusion.31), channel_id=1, replica_groups=mesh['kv'=8,'tp'=4] {'tp'}, use_global_device_ids=true, to_apply=%region_11.12 | all-reduce | flops 32 | bytes 256 | tf_op jit(solution)/shard_map/psum | solution.py:18
  212.9 0.8 fusion.33
  213.8 31.4 %all_gather.18 = bf16[256,512]{1,0:T(8,128)(2,1)S(1)} all-gather(bf16[32,512]{1,0:T(8,128)(2,1)S(1)} %fusion.33), channel_id=1, replica_groups=mesh['kv'=8,'tp'=4] {'kv'}, dimensions={0}, use_global_device_ids=true | all-gather | bytes 294912 | tf_op jit(solution)/shard_map/all_gather | solution.py:22
  245.1 1.5 convolution_convert_fusion.1
  246.6 1.5 convolution_convert_fusion.2
  248.2 1.1 copy.49
  249.3 0.0 reduce-scatter.18.cloned.1.call-update
  249.4 0.0 reduce-scatter.14.cloned.1.call-start
  249.4 0.1 copy.43
  249.5 0.1 copy.44
  249.6 0.1 reshape.77
  249.6 0.1 broadcast_multiply_fusion
  249.7 22.4 %reduce-scatter.18.cloned.1.call-done = bf16[64,1408]{1,0:T(8,128)(2,1)} async-done(((bf16[256,1408]{1,0:T(8,128)(2,1)}), bf16[64,1408]{1,0:T(8,128)(2,1)}) %reduce-scatter.18.cloned.1.call-update) | async-done | bytes 180240 | tf_op jit(solution)/shard_map/reduce_scatter | solution.py:31
  272.2 0.9 convert_element_type.189
  273.1 0.1 fusion.22
  273.2 6.1 %all_gather.19 = bf16[256,704]{1,0:T(8,128)(2,1)S(1)} all-gather(bf16[64,704]{1,0:T(8,128)(2,1)S(1)} %fusion.22), channel_id=1, replica_groups=mesh['kv'=8,'tp'=4] {'tp'}, dimensions={0}, use_global_device_ids=true | all-gather | bytes 450560 | tf_op jit(solution)/shard_map/all_gather | solution.py:35
  279.4 2.2 convolution_convert_fusion.5
  281.6 0.0 reduce-scatter.14.cloned.1.call-update
  281.6 8.5 %multiply_add_fusion = f32[32,8,64,128]{3,2,1,0:T(8,128)} fusion(f32[32,8,64,128]{3,2,1,0:T(8,128)} %param.47, f32[32,8,128]{2,1,0:T(8,128)S(1)} %bitcast.34, f32[32,8,64]{2,1,0:T(8,128)S(1)} %broadcast_multiply_fusion, f32[32,8]{1,0:T(8,128)S(1)} %copy.43), kind=kLoop, calls=%fused_computation | loop fusion | flops 6291456 | bytes 16974848 | tf_op jit(solution)/shard_map/add | solution.py:103
  290.1 54.4 %reduce-scatter.14.cloned.1.call-done = bf16[32,512]{1,0:T(8,128)(2,1)} async-done(((bf16[256,512]{1,0:T(8,128)(2,1)}), bf16[32,512]{1,0:T(8,128)(2,1)}) %reduce-scatter.14.cloned.1.call-update) | async-done | bytes 32784 | tf_op jit(solution)/shard_map/reduce_scatter | solution.py:36
  344.5 1.4 fusion.34
  (55 shorter events, 0.4 us)
Async XLA Ops:
  7.2 179.2 %copy-start = (bf16[512,2048]{1,0:T(8,128)(2,1)S(1)}, bf16[512,2048]{1,0:T(8,128)(2,1)}, u32[]{:S(2)}) copy-start(bf16[512,2048]{1,0:T(8,128)(2,1)} %param.49) | copy-start | bytes 6291460
  7.2 141.9 %copy-start.1 = (bf16[32,512]{1,0:T(8,128)(2,1)S(1)}, bf16[32,512]{1,0:T(8,128)(2,1)}, u32[]{:S(2)}) copy-start(bf16[32,512]{1,0:T(8,128)(2,1)} %param.27) | copy-start | bytes 98308
  7.2 78.8 %copy-start.7 = (bf16[4,256]{1,0:T(4,128)(2,1)S(1)}, bf16[4,256]{1,0:T(4,128)(2,1)}, u32[]{:S(2)}) copy-start(bf16[4,256]{1,0:T(4,128)(2,1)} %param.42) | copy-start | bytes 6148
  7.2 78.9 %copy-start.8 = (bf16[4,256]{1,0:T(4,128)(2,1)S(1)}, bf16[4,256]{1,0:T(4,128)(2,1)}, u32[]{:S(2)}) copy-start(bf16[4,256]{1,0:T(4,128)(2,1)} %param.43) | copy-start | bytes 6148
  7.2 78.9 %copy-start.6 = (bf16[4,512]{1,0:T(4,128)(2,1)S(1)}, bf16[4,512]{1,0:T(4,128)(2,1)}, u32[]{:S(2)}) copy-start(bf16[4,512]{1,0:T(4,128)(2,1)} %param.41) | copy-start | bytes 12292
  7.2 78.9 %copy-start.13 = (f32[8]{0:T(128)S(1)}, f32[8]{0:T(128)}, u32[]{:S(2)}) copy-start(f32[8]{0:T(128)} %param.39) | copy-start | bytes 100
  7.2 78.9 %copy-start.14 = (f32[8]{0:T(128)S(1)}, f32[8]{0:T(128)}, u32[]{:S(2)}) copy-start(f32[8]{0:T(128)} %param.40) | copy-start | bytes 100
  7.2 79.0 %copy-start.10 = (bf16[512]{0:T(512)(128)(2,1)S(1)}, bf16[512]{0:T(512)(128)(2,1)}, u32[]{:S(2)}) copy-start(bf16[512]{0:T(512)(128)(2,1)} %param.48) | copy-start | bytes 3076
  7.3 79.0 %copy-start.9 = (bf16[2048]{0:T(1024)(128)(2,1)S(1)}, bf16[2048]{0:T(1024)(128)(2,1)}, u32[]{:S(2)}) copy-start(bf16[2048]{0:T(1024)(128)(2,1)} %param.32) | copy-start | bytes 12292
  7.3 79.0 %copy-start.4 = (bf16[32,3,256]{2,0,1:T(8,128)(2,1)S(1)}, bf16[32,3,256]{2,0,1:T(8,128)(2,1)}, u32[]{:S(2)}) copy-start(bf16[32,3,256]{2,0,1:T(8,128)(2,1)} %param.46) | copy-start | bytes 147460
  7.3 79.0 %copy-start.5 = (bf16[32,3,256]{2,0,1:T(8,128)(2,1)S(1)}, bf16[32,3,256]{2,0,1:T(8,128)(2,1)}, u32[]{:S(2)}) copy-start(bf16[32,3,256]{2,0,1:T(8,128)(2,1)} %param.45) | copy-start | bytes 147460
  7.3 79.1 %copy-start.3 = (bf16[32,3,512]{2,0,1:T(8,128)(2,1)S(1)}, bf16[32,3,512]{2,0,1:T(8,128)(2,1)}, u32[]{:S(2)}) copy-start(bf16[32,3,512]{2,0,1:T(8,128)(2,1)} %param.44) | copy-start | bytes 294916
  7.3 153.4 %copy-start.15 = (f32[8]{0:T(128)S(1)}, f32[8]{0:T(128)}, u32[]{:S(2)}) copy-start(f32[8]{0:T(128)} %param.38) | copy-start | bytes 100
  7.3 153.4 %copy-start.12 = (bf16[2048,8]{0,1:T(8,128)(2,1)S(1)}, bf16[2048,8]{0,1:T(8,128)(2,1)}, u32[]{:S(2)}) copy-start(bf16[2048,8]{0,1:T(8,128)(2,1)} %param.37) | copy-start | bytes 98308
  7.3 69.3 %reduce-scatter.16.cloned.1.call-start = ((), (), s32[]{:S(2)}) async-start(), calls=%async_computation.8 | async-start | bytes 901120 | tf_op jit(solution)/shard_map/reduce_scatter | solution.py:31
  53.8 95.3 %reduce-scatter.10.cloned.1.call-start = ((), (), s32[]{:S(2)}) async-start(), calls=%async_computation.5 | async-start | bytes 294912 | tf_op jit(solution)/shard_map/reduce_scatter | solution.py:36
  86.0 120.3 %reduce-scatter.12.cloned.1.call-start = ((), (), s32[]{:S(2)}) async-start(), calls=%async_computation.6 | async-start | bytes 163840 | tf_op jit(solution)/shard_map/reduce_scatter | solution.py:123
  160.8 26.8 %copy-start.11 = (bf16[512]{0:T(512)(128)(2,1)S(1)}, bf16[512]{0:T(512)(128)(2,1)}, u32[]{:S(2)}) copy-start(bf16[512]{0:T(512)(128)(2,1)} %param.50) | copy-start | bytes 3076
  187.5 84.7 %reduce-scatter.18.cloned.1.call-start = ((), (), s32[]{:S(2)}) async-start(), calls=%async_computation.9 | async-start | bytes 901120 | tf_op jit(solution)/shard_map/reduce_scatter | solution.py:31
  249.4 95.1 %reduce-scatter.14.cloned.1.call-start = ((), (), s32[]{:S(2)}) async-start(), calls=%async_computation.7 | async-start | bytes 294912 | tf_op jit(solution)/shard_map/reduce_scatter | solution.py:36
  281.6 62.9 %copy-start.2 = (bf16[32,512]{1,0:T(8,128)(2,1)S(1)}, bf16[32,512]{1,0:T(8,128)(2,1)}, u32[]{:S(2)}) copy-start(bf16[32,512]{1,0:T(8,128)(2,1)} %reduce-scatter.12.cloned.1.call-done) | copy-start | bytes 98308
Sparse Core Ops, SparseCore 0:
  53.9 22.6 reduce-scatter.15
  86.1 62.9 reduce-scatter.9
  187.6 18.6 reduce-scatter.11
  249.5 22.6 reduce-scatter.17
  281.7 62.7 reduce-scatter.13
where the time goes:
time: 353 us; the launch traced here: 352 us
  waiting for transfers between devices  181 us (51%)
  blocking collectives  94.4 us (27%)
  matrix products  41.1 us (12%)
  other arithmetic  18 us (5%)
  between operations  14.3 us (4%)
    reduce_scatter x2, waiting for transfers between devices, half_step(): lax.psum_scatter(jnp.dot(hidden, down_weight, preferred_element_type=jnp....  117 us
    all_gather x2, blocking collectives, half_step(): row_piece = lax.all_gather(normed, 'kv', axis=0, tiled=True)  62.6 us
    reduce_scatter x2, waiting for transfers between devices, half_step(): lax.psum_scatter(partial_value.astype(jnp.bfloat16), 'tp', scatter_dimens...  45.2 us
    dot_general x1, matrix products, state_mixer(): jnp.einsum('bgrpn,bgn->bgrp', updated, read_groups, precision=lax.Precisi...  22 us
    reduce_scatter x1, waiting for transfers between devices, state_mixer(): lax.psum_scatter(partial_out.astype(jnp.bfloat16), 'tp', scatter_dimensio...  18.7 us
    psum x2, blocking collectives, half_step(): row_total = lax.psum(jnp.sum(widened * widened, axis=1), 'tp')  14.1 us
    all_gather x2, blocking collectives, half_step(): hidden = lax.all_gather(active, 'tp', axis=0, tiled=True)  12.3 us
    add x1, other arithmetic, state_mixer(): retain_g[..., None, None] * old_state  8.5 us
  transfers between devices with their start and end apart: 5, of which 5 were waited for; matrix products, arithmetic and copies ran while one was open for 3% of the time, Pallas kernels for 0%

commit v1 on v0

--- a/solution.py
+++ b/solution.py
@@ -19,7 +19,9 @@
     factor = lax.rsqrt(row_total / D + norm_eps)
     normed = (widened * factor[:, None] * gain.astype(jnp.float32)[None, :]).astype(jnp.bfloat16)
     hidden_cols = gate_weight.shape[1]
-    row_piece = lax.all_gather(normed, "kv", axis=0, tiled=True)
+    row_piece = jnp.concatenate(
+        lax.all_to_all(jnp.stack([normed] * lax.axis_size("kv")), "kv", 0, 0), axis=0
+    )
     gate_part = jnp.dot(row_piece, gate_weight, preferred_element_type=jnp.float32).astype(
         jnp.bfloat16
     )

time: 353 us -> 315 us (0.89)
  blocking collectives: 94.4 us -> 59.9 us
  waiting for transfers between devices: 181 us -> 174 us
    all_gather x2 -> x0, blocking collectives: 62.6 us -> none  [half_step(): row_piece = lax.all_gather(normed, 'kv', axis=0, tiled=True)]
    all_to_all x0 -> x2, blocking collectives: none -> 28 us  [half_step(): lax.all_to_all(jnp.stack([normed] * lax.axis_size('kv')), 'kv', 0, 0)]
    reduce_scatter x2, waiting for transfers between devices: 117 us -> 113 us  [half_step(): lax.psum_scatter(jnp.dot(hidden, down_weight, preferred_element_type=jnp....]
  transfers between devices with their start and end apart: 5 -> 5, of which waited for: 5 -> 5; matrix products, arithmetic and copies ran while one was open for 3% -> 4% of each run, Pallas kernels for 0% -> 0%
where the time goes in v1:
time: 315 us; the launch traced here: 314 us
  waiting for transfers between devices  174 us (55%)
  blocking collectives  59.9 us (19%)
  matrix products  39.9 us (13%)
  other arithmetic  21.2 us (7%)
  between operations  14.1 us (4%)
  local copies, waits for them, and re-layouts  4.73 us (2%)
    reduce_scatter x2, waiting for transfers between devices, half_step(): lax.psum_scatter(jnp.dot(hidden, down_weight, preferred_element_type=jnp....  113 us
    reduce_scatter x2, waiting for transfers between devices, half_step(): lax.psum_scatter(partial_value.astype(jnp.bfloat16), 'tp', scatter_dimens...  42.1 us
    all_to_all x2, blocking collectives, half_step(): lax.all_to_all(jnp.stack([normed] * lax.axis_size('kv')), 'kv', 0, 0)  28 us
    dot_general x1, matrix products, state_mixer(): jnp.einsum('bgrpn,bgn->bgrp', updated, read_groups, precision=lax.Precisi...  22 us
    reduce_scatter x1, waiting for transfers between devices, state_mixer(): lax.psum_scatter(partial_out.astype(jnp.bfloat16), 'tp', scatter_dimensio...  18.7 us
    psum x2, blocking collectives, half_step(): row_total = lax.psum(jnp.sum(widened * widened, axis=1), 'tp')  14.1 us
    all_gather x2, blocking collectives, half_step(): hidden = lax.all_gather(active, 'tp', axis=0, tiled=True)  12.3 us
    add x1, other arithmetic, state_mixer(): retain_g[..., None, None] * old_state  8.5 us
  transfers between devices with their start and end apart: 5, of which 5 were waited for; matrix products, arithmetic and copies ran while one was open for 4% of the time, Pallas kernels for 0%

profile of v1, /device:TPU:0, one launch (start us, length us, event | category | flops | bytes accessed | tf_op | source)
XLA Modules:
  0.0 313.6 jit_solution(5556013366093624469)
XLA Ops:
  7.2 0.0 reduce-scatter.16.cloned.1.call-start
  7.3 1.0 fusion.27
  8.3 8.4 %psum.14 = f32[32]{0:T(128)S(1)} all-reduce(f32[32]{0:T(128)S(1)} %fusion.27), channel_id=1, replica_groups=mesh['kv'=8,'tp'=4] {'tp'}, use_global_device_ids=true, to_apply=%region_1.0 | all-reduce | flops 32 | bytes 256 | tf_op jit(solution)/shard_map/psum | solution.py:18
  16.7 0.7 convert_element_type.148
  17.4 0.8 fusion.29
  18.2 13.9 %all_to_all.10 = bf16[8,32,512]{2,1,0:T(8,128)(2,1)S(1)} all-to-all(bf16[8,32,512]{2,1,0:T(8,128)(2,1)S(1)} %stack.4), channel_id=1, replica_groups=mesh['kv'=8,'tp'=4] {'kv'}, dimensions={0} | all-to-all | bytes 524288 | tf_op jit(solution)/shard_map/all_to_all | solution.py:23
  32.1 1.5 convolution_convert_fusion.3
  33.6 1.5 convolution_convert_fusion.4
  35.1 1.1 copy.47
  36.3 0.0 reduce-scatter.10.cloned.1.call-start
  36.3 21.4 %reduce-scatter.16.cloned.1.call-done = bf16[64,1408]{1,0:T(8,128)(2,1)} async-done(((bf16[256,1408]{1,0:T(8,128)(2,1)}), bf16[64,1408]{1,0:T(8,128)(2,1)}) %reduce-scatter.16.cloned.1.call-update) | async-done | bytes 180240 | tf_op jit(solution)/shard_map/reduce_scatter | solution.py:33
  57.8 0.9 convert_element_type.152
  58.7 0.1 fusion.23
  58.9 6.1 %all_gather.9 = bf16[256,704]{1,0:T(8,128)(2,1)S(1)} all-gather(bf16[64,704]{1,0:T(8,128)(2,1)S(1)} %fusion.23), channel_id=1, replica_groups=mesh['kv'=8,'tp'=4] {'tp'}, dimensions={0}, use_global_device_ids=true | all-gather | bytes 450560 | tf_op jit(solution)/shard_map/all_gather | solution.py:37
  65.0 1.1 convolution_convert_fusion.6
  66.1 0.0 reduce-scatter.12.cloned.1.call-start
  66.3 0.7 exp.38
  66.9 0.7 mul.301
  67.7 0.7 convert_element_type.179
  68.4 0.8 multiply_reduce_fusion.1
  69.2 0.8 multiply_reduce_fusion.2
  70.0 0.9 multiply_reduce_fusion
  70.9 58.4 %reduce-scatter.10.cloned.1.call-done = bf16[32,512]{1,0:T(8,128)(2,1)} async-done(((bf16[256,512]{1,0:T(8,128)(2,1)}), bf16[32,512]{1,0:T(8,128)(2,1)}) %reduce-scatter.10.cloned.1.call-update) | async-done | bytes 32784 | tf_op jit(solution)/shard_map/reduce_scatter | solution.py:38
  129.3 0.8 fusion.30
  130.1 5.4 %all_gather.10 = bf16[32,2048]{1,0:T(8,128)(2,1)S(1)} all-gather(bf16[32,512]{1,0:T(8,128)(2,1)S(1)} %fusion.30), channel_id=1, replica_groups=mesh['kv'=8,'tp'=4] {'tp'}, dimensions={1}, use_global_device_ids=true | all-gather | bytes 163840 | tf_op jit(solution)/shard_map/all_gather | solution.py:76
  135.5 0.1 fusion.19
  135.6 1.6 divide_multiply_fusion.3
  137.2 1.6 divide_multiply_fusion.2
  138.8 2.1 fusion.7
  141.0 0.2 multiply_exponential_fusion
  141.2 0.1 copy.41
  141.3 0.1 copy.40
  141.4 2.1 divide_multiply_fusion.1
  143.6 0.1 reshape.84
  143.7 0.1 broadcast_multiply_fusion.1
  143.8 22.0 %fusion = f32[32,2,1,4,64]{4,2,3,1,0:T(1,128)S(1)} fusion(f32[32,2,128,1,1]{2,3,4,1,0:T(1,128)S(1)} %bitcast.44, f32[32,2,4,64,128]{4,3,2,1,0:T(8,128)} %bitcast.35, f32[32,2,128]{2,1,0:T(2,128)S(1)} %mul.292, f32[32,2,4,64]{3,2,1,0:T(4,128)S(1)} %broadcast_multiply_fusion.1, f32[32,2,4]{2,1,0:T(2,128)S(1)} %copy.40), kind=kOutput, calls=%fused_computation.1 | convolution fusion | flops 31457280 | bytes 8586240 | tf_op jit(solution)/shard_map/bgrpn,bgn->bgrp/dot_general | solution.py:108
  165.8 0.1 add_convert_fusion
  165.9 0.1 reshape.86
  166.1 0.1 reshape.87
  166.2 0.2 fusion.26
  166.4 0.1 mul.309
  166.6 1.1 convolution_convert_fusion
  167.7 0.0 reduce-scatter.18.cloned.1.call-start
  167.8 18.7 %reduce-scatter.12.cloned.1.call-done = bf16[32,512]{1,0:T(8,128)(2,1)} async-done(((bf16[32,2048]{1,0:T(8,128)(2,1)}), bf16[32,512]{1,0:T(8,128)(2,1)}) %reduce-scatter.12.cloned.1.call-update) | async-done | bytes 32784 | tf_op jit(solution)/shard_map/reduce_scatter | solution.py:125
  186.5 0.9 fusion.31
  187.4 5.8 %psum.15 = f32[32]{0:T(128)S(1)} all-reduce(f32[32]{0:T(128)S(1)} %fusion.31), channel_id=1, replica_groups=mesh['kv'=8,'tp'=4] {'tp'}, use_global_device_ids=true, to_apply=%region_11.12 | all-reduce | flops 32 | bytes 256 | tf_op jit(solution)/shard_map/psum | solution.py:18
  193.1 0.8 fusion.33
  194.0 14.2 %all_to_all.11 = bf16[8,32,512]{2,1,0:T(8,128)(2,1)S(1)} all-to-all(bf16[8,32,512]{2,1,0:T(8,128)(2,1)S(1)} %stack.5), channel_id=1, replica_groups=mesh['kv'=8,'tp'=4] {'kv'}, dimensions={0} | all-to-all | bytes 524288 | tf_op jit(solution)/shard_map/all_to_all | solution.py:23
  208.2 1.5 convolution_convert_fusion.1
  209.7 1.5 convolution_convert_fusion.2
  211.2 1.1 copy.49
  212.4 0.0 reduce-scatter.14.cloned.1.call-start
  212.4 0.1 copy.43
  212.5 0.1 copy.44
  212.6 0.1 reshape.89
  212.7 0.1 broadcast_multiply_fusion
  212.8 20.6 %reduce-scatter.18.cloned.1.call-done = bf16[64,1408]{1,0:T(8,128)(2,1)} async-done(((bf16[256,1408]{1,0:T(8,128)(2,1)}), bf16[64,1408]{1,0:T(8,128)(2,1)}) %reduce-scatter.18.cloned.1.call-update) | async-done | bytes 180240 | tf_op jit(solution)/shard_map/reduce_scatter | solution.py:33
  233.4 0.9 convert_element_type.189
  234.4 0.1 fusion.22
  234.5 6.1 %all_gather.11 = bf16[256,704]{1,0:T(8,128)(2,1)S(1)} all-gather(bf16[64,704]{1,0:T(8,128)(2,1)S(1)} %fusion.22), channel_id=1, replica_groups=mesh['kv'=8,'tp'=4] {'tp'}, dimensions={0}, use_global_device_ids=true | all-gather | bytes 450560 | tf_op jit(solution)/shard_map/all_gather | solution.py:37
  240.6 2.2 convolution_convert_fusion.5
  242.9 8.5 %multiply_add_fusion = f32[32,8,64,128]{3,2,1,0:T(8,128)} fusion(f32[32,8,64,128]{3,2,1,0:T(8,128)} %param.47, f32[32,8,128]{2,1,0:T(8,128)S(1)} %bitcast.40, f32[32,8,64]{2,1,0:T(8,128)S(1)} %broadcast_multiply_fusion, f32[32,8]{1,0:T(8,128)S(1)} %copy.43), kind=kLoop, calls=%fused_computation | loop fusion | flops 6291456 | bytes 16974848 | tf_op jit(solution)/shard_map/add | solution.py:105
  251.4 54.4 %reduce-scatter.14.cloned.1.call-done = bf16[32,512]{1,0:T(8,128)(2,1)} async-done(((bf16[256,512]{1,0:T(8,128)(2,1)}), bf16[32,512]{1,0:T(8,128)(2,1)}) %reduce-scatter.14.cloned.1.call-update) | async-done | bytes 32784 | tf_op jit(solution)/shard_map/reduce_scatter | solution.py:38
  305.7 1.4 fusion.34
  (45 shorter events, 0.4 us)
Async XLA Ops:
  7.2 159.4 %copy-start = (bf16[512,2048]{1,0:T(8,128)(2,1)S(1)}, bf16[512,2048]{1,0:T(8,128)(2,1)}, u32[]{:S(2)}) copy-start(bf16[512,2048]{1,0:T(8,128)(2,1)} %param.49) | copy-start | bytes 6291460
  7.2 57.8 %copy-start.1 = (bf16[704,512]{1,0:T(8,128)(2,1)S(1)}, bf16[704,512]{1,0:T(8,128)(2,1)}, u32[]{:S(2)}) copy-start(bf16[704,512]{1,0:T(8,128)(2,1)} %param.31) | copy-start | bytes 2162692
  7.2 59.0 %copy-start.4 = (bf16[4,256]{1,0:T(4,128)(2,1)S(1)}, bf16[4,256]{1,0:T(4,128)(2,1)}, u32[]{:S(2)}) copy-start(bf16[4,256]{1,0:T(4,128)(2,1)} %param.42) | copy-start | bytes 6148
  7.2 59.0 %copy-start.5 = (bf16[4,256]{1,0:T(4,128)(2,1)S(1)}, bf16[4,256]{1,0:T(4,128)(2,1)}, u32[]{:S(2)}) copy-start(bf16[4,256]{1,0:T(4,128)(2,1)} %param.43) | copy-start | bytes 6148
  7.2 59.0 %copy-start.3 = (bf16[4,512]{1,0:T(4,128)(2,1)S(1)}, bf16[4,512]{1,0:T(4,128)(2,1)}, u32[]{:S(2)}) copy-start(bf16[4,512]{1,0:T(4,128)(2,1)} %param.41) | copy-start | bytes 12292
  7.2 61.1 %copy-start.6 = (bf16[2048]{0:T(1024)(128)(2,1)S(1)}, bf16[2048]{0:T(1024)(128)(2,1)}, u32[]{:S(2)}) copy-start(bf16[2048]{0:T(1024)(128)(2,1)} %param.32) | copy-start | bytes 12292
  7.2 50.6 %reduce-scatter.16.cloned.1.call-start = ((), (), s32[]{:S(2)}) async-start(), calls=%async_computation.10 | async-start | bytes 901120 | tf_op jit(solution)/shard_map/reduce_scatter | solution.py:33
  36.3 104.7 %copy-start.8 = (bf16[2048,8]{0,1:T(8,128)(2,1)S(1)}, bf16[2048,8]{0,1:T(8,128)(2,1)}, u32[]{:S(2)}) copy-start(bf16[2048,8]{0,1:T(8,128)(2,1)} %param.37) | copy-start | bytes 98308
  36.3 104.7 %copy-start.9 = (f32[8]{0:T(128)S(1)}, f32[8]{0:T(128)}, u32[]{:S(2)}) copy-start(f32[8]{0:T(128)} %param.38) | copy-start | bytes 100
  36.3 93.0 %reduce-scatter.10.cloned.1.call-start = ((), (), s32[]{:S(2)}) async-start(), calls=%async_computation.7 | async-start | bytes 294912 | tf_op jit(solution)/shard_map/reduce_scatter | solution.py:38
  66.1 120.4 %reduce-scatter.12.cloned.1.call-start = ((), (), s32[]{:S(2)}) async-start(), calls=%async_computation.8 | async-start | bytes 163840 | tf_op jit(solution)/shard_map/reduce_scatter | solution.py:125
  140.9 26.8 %copy-start.7 = (bf16[512]{0:T(512)(128)(2,1)S(1)}, bf16[512]{0:T(512)(128)(2,1)}, u32[]{:S(2)}) copy-start(bf16[512]{0:T(512)(128)(2,1)} %param.50) | copy-start | bytes 3076
  167.7 65.7 %reduce-scatter.18.cloned.1.call-start = ((), (), s32[]{:S(2)}) async-start(), calls=%async_computation.11 | async-start | bytes 901120 | tf_op jit(solution)/shard_map/reduce_scatter | solution.py:33
  212.4 93.3 %reduce-scatter.14.cloned.1.call-start = ((), (), s32[]{:S(2)}) async-start(), calls=%async_computation.9 | async-start | bytes 294912 | tf_op jit(solution)/shard_map/reduce_scatter | solution.py:38
  242.9 62.9 %copy-start.2 = (bf16[32,512]{1,0:T(8,128)(2,1)S(1)}, bf16[32,512]{1,0:T(8,128)(2,1)}, u32[]{:S(2)}) copy-start(bf16[32,512]{1,0:T(8,128)(2,1)} %reduce-scatter.12.cloned.1.call-done) | copy-start | bytes 98308
Sparse Core Ops, SparseCore 0:
  36.4 21.3 reduce-scatter.15
  66.2 62.9 reduce-scatter.9
  167.8 18.6 reduce-scatter.11
  212.5 20.8 reduce-scatter.17
  242.9 62.7 reduce-scatter.13
